TPU v7x, 512 devices: a whole 4x4x16 slice. The times are simulated.
512 devices in a mesh: ep: 128 (over z, x, core), tp: 4 (over y).
Axes of the slice: x: 4, y: 4, z: 16, core: 2. Of those that a mesh axis runs over, the one named last changes fastest.
Arguments:
- tokens: bfloat16 [512, 2048], P('ep', 'tp'), may hold values from -6 to 6
- norm_gain: bfloat16 [2048], P('tp'), may hold values from 0.099609375 to 1.8984375
- w_query: bfloat16 [2048, 2048], P('tp', 'ep'), may hold values from -0.125 to 0.125
- w_forget: bfloat16 [2048, 2048], P('tp', 'ep'), may hold values from -0.125 to 0.125
- w_input: bfloat16 [2048, 2048], P('tp', 'ep'), may hold values from -0.125 to 0.125
- forget_floor: float32 [2048], P('tp'), may hold values from 0 to 0.9
- head_gain: bfloat16 [128], replicated, may hold values from 0.099609375 to 1.8984375
- w_output: bfloat16 [2048, 2048], P('tp', 'ep'), may hold values from -0.125 to 0.125
- state: float32 [512, 16, 128, 128], P('ep', 'tp'), may hold values from -6 to 6
- ffn_gain: bfloat16 [2048], P('tp'), may hold values from 0.099609375 to 1.8984375
- route_experts: int32 [512, 2], P('ep'), may hold values from 0 to 7, all different within a row; in each aligned block of 4 rows (0 to 3, 4 to 7, ...) at most 2 rows name the same one
- route_weights: float32 [512, 2], P('ep'), may hold values from 0.1 to 1
- w_gate: bfloat16 [128, 2048, 448], P('ep', None, 'tp'), may hold values from -0.125 to 0.125
- w_up: bfloat16 [128, 2048, 448], P('ep', None, 'tp'), may hold values from -0.125 to 0.125
- w_down: bfloat16 [128, 448, 2048], P('ep', 'tp'), may hold values from -0.0625 to 0.0625
Outputs:
- mixed: bfloat16 [512, 2048], P('ep', 'tp')
- new_state: float32 [512, 16, 128, 128], P('ep', 'tp')
Inputs may be any that keep to these rules, and one draw needn't show every extreme that they name: `route_experts`: each row names two different experts. Among the rows of one index of ep, no expert is named by more than 2 rows, and in every draw some expert is named by exactly 2 of them.
All inputs are finite; a program needn't handle non-finite values.
Results may differ from a plain program's by a relative error of at most 0.014.
Values may be sent and summed in bfloat16 or wider, within the bound.
No kernel may reach another device: no remote copies, remote signals or barrier semaphores. Data moves between devices by JAX's collectives and lax.ppermute only.
A program may use at most 64 MiB of HBM per device.

v0:
```python
import jax
import jax.numpy as jnp
from jax import lax
from jax.sharding import Mesh
from jax.sharding import PartitionSpec as P

EXPERTS = 8
EP = ("ep_0", "ep_1", "ep_2")
EPS = 1e-06


def laid_out(blocks, dim):
    blocks = jnp.moveaxis(blocks, 0, dim)
    dims = blocks.shape
    return blocks.reshape(*dims[:dim], dims[dim] * dims[dim + 1], *dims[dim + 2 :])


def all_blocks(shard, axes, sequence):
    blocks = shard
    for k in sequence:
        blocks = lax.all_gather(blocks, axes[k])
    done = sequence[::-1]
    back = [done.index(k) for k in range(len(axes))]
    blocks = blocks.transpose(*back, *range(len(axes), blocks.ndim))
    return blocks.reshape(-1, *shard.shape)


def whole_of(shard, axes, sequence, dim):
    return laid_out(all_blocks(shard, axes, sequence), dim)


def in_blocks(shard, dim, length):
    before, after = (shard.shape[:dim], shard.shape[dim + 1 :])
    return jnp.moveaxis(shard.reshape(*before, length, -1, *after), dim, 0)


def sent_and_summed(shard, axis, dim):
    length = lax.axis_size(axis)
    blocks = lax.all_to_all(in_blocks(shard, dim, length), axis, 0, 0, tiled=True)
    return jnp.sum(blocks, axis=0)


def summed_on_arrival(shard, axis, dim):
    blocks = in_blocks(shard, dim, lax.axis_size(axis))
    arrived = lax.all_to_all(blocks, axis, split_axis=0, concat_axis=0, tiled=True)
    return arrived.astype(jnp.float32).sum(axis=0)


def shards(
    tokens,
    norm_gain,
    w_query,
    w_forget,
    w_input,
    forget_floor,
    head_gain,
    w_output,
    state,
    ffn_gain,
    route_experts,
    route_weights,
    w_gate,
    w_up,
    w_down,
):
    ep_count = lax.axis_size(EP)
    tp_count = lax.axis_size("tp")
    seq_count = tokens.shape[0]
    model_width = tokens.shape[1] * tp_count
    head_size = state.shape[2]
    local_heads = state.shape[1]
    tok_f32 = tokens.astype(jnp.float32)
    sum_sq = lax.psum(jnp.sum(tok_f32 * tok_f32, axis=1), "tp")
    normed = (
        tok_f32 * lax.rsqrt(sum_sq / model_width + EPS)[:, None] * norm_gain.astype(jnp.float32)
    ).astype(jnp.bfloat16)
    w_joint = jnp.concatenate([w_query, w_forget, w_input], axis=1)
    partial_value = jnp.dot(
        whole_of(normed, EP, (1, 0, 2), 0), w_joint, preferred_element_type=jnp.float32
    )
    moved_in = lax.all_to_all(partial_value, EP, split_axis=0, concat_axis=1, tiled=True)
    summed = sent_and_summed(moved_in, "tp", 1)
    col_count = w_query.shape[1]
    blocks = summed.reshape(seq_count, -1, 3, col_count)
    queries = blocks[:, :, 0, :].reshape(seq_count, local_heads, head_size)
    fgate = blocks[:, :, 1, :].reshape(seq_count, local_heads, head_size)
    inputs = blocks[:, :, 2, :].reshape(seq_count, local_heads, head_size)
    floors = forget_floor.reshape(local_heads, head_size)
    forget = floors + (1.0 - floors) * jax.nn.sigmoid(fgate)
    new_state = forget[..., None] * state + (1.0 - forget)[..., None] * inputs[:, :, None, :]
    reads = jnp.einsum(
        "bhk,bhkv->bhv", jax.nn.silu(queries), new_state, precision=lax.Precision.HIGHEST
    )
    head_sq = jnp.mean(reads * reads, axis=-1, keepdims=True)
    heads_out = (
        (reads * lax.rsqrt(head_sq + EPS) * head_gain.astype(jnp.float32))
        .reshape(seq_count, local_heads * head_size)
        .astype(jnp.bfloat16)
    )
    part_out = jnp.dot(
        whole_of(heads_out, EP, (1, 0, 2), 0), w_output, preferred_element_type=jnp.float32
    )
    moved_out = lax.all_to_all(
        part_out.astype(jnp.bfloat16), EP, split_axis=0, concat_axis=1, tiled=True
    ).astype(part_out.dtype)
    mixer_slice = summed_on_arrival(moved_out.astype(jnp.bfloat16), "tp", 1).astype(jnp.bfloat16)
    middle = (tok_f32 + mixer_slice.astype(jnp.float32)).astype(jnp.bfloat16)
    middle_f32 = middle.astype(jnp.float32)
    span_count = ep_count // EXPERTS
    capacity = max(2, seq_count // 2)
    positions = jnp.arange(seq_count, dtype=jnp.int32)
    earlier = positions[None, :] < positions[:, None]
    same_expert = route_experts[:, :, None, None] == route_experts[None, None, :, :]
    slot_rank = jnp.sum(same_expert & earlier[:, None, :, None], axis=(2, 3))
    owners = jnp.arange(ep_count, dtype=jnp.int32) // span_count
    matched = route_experts[None, :, :] == owners[:, None, None]
    placed = slot_rank[:, :, None] == jnp.arange(capacity, dtype=jnp.int32)[None, None, :]
    slot_hits = matched[:, :, :, None] & placed[None, :, :, :]
    chosen = jnp.sum(slot_hits.astype(jnp.float32), axis=2).astype(jnp.bfloat16)
    weight_hits = jnp.sum(slot_hits.astype(jnp.float32) * route_weights[None, :, :, None], axis=2)
    row_stat = lax.psum(jnp.sum(middle_f32 * middle_f32, axis=1), "tp")
    second = (
        middle_f32 * lax.rsqrt(row_stat / model_width + EPS)[:, None] * ffn_gain.astype(jnp.float32)
    ).astype(jnp.bfloat16)
    outgoing = jnp.einsum("pts,td->psd", chosen, second, preferred_element_type=jnp.float32).astype(
        jnp.bfloat16
    )
    arrived_part = lax.all_to_all(outgoing, EP, split_axis=0, concat_axis=0, tiled=True)
    arrived = lax.all_gather(arrived_part, "tp", axis=2, tiled=True)
    expert_rows = arrived.reshape(ep_count * capacity, model_width)
    gate_act = jnp.dot(expert_rows, w_gate[0], preferred_element_type=jnp.float32)
    up_act = jnp.dot(expert_rows, w_up[0], preferred_element_type=jnp.float32)
    hidden = (jax.nn.silu(gate_act) * up_act).astype(jnp.bfloat16)
    piece_out = jnp.dot(hidden, w_down[0], preferred_element_type=jnp.float32)
    piece_total = summed_on_arrival(piece_out.astype(jnp.bfloat16), "tp", 1)
    returned = lax.all_to_all(
        piece_total.reshape(ep_count, capacity, -1).astype(jnp.bfloat16),
        EP,
        split_axis=0,
        concat_axis=0,
        tiled=True,
    ).astype(jnp.float32)
    routed = jnp.einsum("pts,psd->td", weight_hits, returned, precision=lax.Precision.HIGHEST)
    result = (middle_f32 + routed).astype(jnp.bfloat16)
    return (result, new_state)


def solution(mesh):
    torus = Mesh(mesh.devices.reshape(16, 4, 2, mesh.shape["tp"]), ("ep_0", "ep_1", "ep_2", "tp"))
    in_specs = (
        P(EP, "tp"),
        P("tp"),
        P("tp", EP),
        P("tp", EP),
        P("tp", EP),
        P("tp"),
        P(),
        P("tp", EP),
        P(EP, "tp", None, None),
        P("tp"),
        P(EP, None),
        P(EP, None),
        P(EP, None, "tp"),
        P(EP, None, "tp"),
        P(EP, "tp", None),
    )
    out_specs = (P(EP, "tp"), P(EP, "tp", None, None))
    return jax.shard_map(
        shards, mesh=torus, in_specs=in_specs, out_specs=out_specs, check_vma=False
    )
```

profile of v0, /device:TPU:33, one launch (start us, length us, event | category | flops | bytes accessed | tf_op | source)
XLA Modules:
  0.0 324.9 jit_solution(1485527307813868062)
XLA Ops:
  8.0 8.7 %psum.14 = f32[4]{0:T(128)S(1)} all-reduce(f32[4]{0:T(128)S(1)} %fusion.22), channel_id=1, replica_groups=mesh['ep_0'=16,'ep_1'=4,'ep_2'=2,'tp'=4] {'tp'}, use_global_device_ids=true, to_apply=%region_1.0 | all-reduce | flops 4 | bytes 32 | tf_op jit(solution)/shard_map/psum | solution.py:73
  18.2 9.5 %all-gather.5 = bf16[4,4,512]{2,1,0:T(4,128)(2,1)S(1)} all-gather(bf16[1,4,512]{2,1,0:T(4,128)(2,1)S(1)} %fusion.31), channel_id=2, replica_groups=mesh['ep_0'=16,'ep_1'=4,'ep_2'=2,'tp'=4] {'ep_1'}, dimensions={0}, use_global_device_ids=true | all-gather | bytes 20480 | tf_op jit(solution)/shard_map/all_gather | solution.py:21
  27.7 27.8 %all-gather.1 = bf16[64,4,512]{2,1,0:T(4,128)(2,1)S(1)} all-gather(bf16[4,4,512]{2,1,0:T(4,128)(2,1)S(1)} %all-gather.5), channel_id=3, replica_groups=mesh['ep_0'=16,'ep_1'=4,'ep_2'=2,'tp'=4] {'ep_0'}, dimensions={0}, use_global_device_ids=true | all-gather | bytes 278528 | tf_op jit(solution)/shard_map/all_gather | solution.py:21
  55.4 14.3 %all-gather.2 = bf16[32,4,4,512]{3,2,1,0:T(4,128)(2,1)S(1)} all-gather(bf16[16,4,4,512]{3,2,1,0:T(4,128)(2,1)S(1)} %bitcast.70), channel_id=4, replica_groups=mesh['ep_0'=16,'ep_1'=4,'ep_2'=2,'tp'=4] {'ep_2'}, dimensions={0}, use_global_device_ids=true | all-gather | bytes 786432 | tf_op jit(solution)/shard_map/all_gather | solution.py:21
  72.2 12.0 %all-to-all-start = ((f32[128,1,192]{2,1,0:T(1,128)}), f32[128,1,192]{2,1,0:T(1,128)S(1)}, u32[]{:S(2)}, u32[]{:S(2)}) async-start(f32[128,1,192]{2,1,0:T(1,128)} %reshape.148), calls=%async_computation | async-start | bytes 262144 | tf_op jit(solution)/shard_map/all_to_all | solution.py:81
  84.4 17.0 %all-to-all-done = f32[128,1,192]{2,1,0:T(1,128)S(1)} async-done(((f32[128,1,192]{2,1,0:T(1,128)}), f32[128,1,192]{2,1,0:T(1,128)S(1)}, u32[]{:S(2)}, u32[]{:S(2)}) %all-to-all-start) | async-done | bytes 98336 | tf_op jit(solution)/shard_map/all_to_all | solution.py:81
  103.9 3.3 %all-to-all-start.1 = ((f32[4,4,1536]{2,1,0:T(4,128)}), f32[4,4,1536]{2,1,0:T(4,128)S(1)}, u32[]{:S(2)}, u32[]{:S(2)}) async-start(f32[4,4,1536]{2,1,0:T(4,128)} %copy.124), calls=%async_computation.1 | async-start | bytes 196608 | tf_op jit(solution)/shard_map/all_to_all | solution.py:39
  107.5 4.4 %all-to-all-done.1 = f32[4,4,1536]{2,1,0:T(4,128)S(1)} async-done(((f32[4,4,1536]{2,1,0:T(4,128)}), f32[4,4,1536]{2,1,0:T(4,128)S(1)}, u32[]{:S(2)}, u32[]{:S(2)}) %all-to-all-start.1) | async-done | bytes 98336 | tf_op jit(solution)/shard_map/all_to_all | solution.py:39
  113.6 1.0 copy-done.1
  114.6 1.0 fusion.38
  115.8 9.1 %all_gather.43 = bf16[4,4,512]{2,1,0:T(4,128)(2,1)S(1)} all-gather(bf16[1,4,512]{2,1,0:T(4,128)(2,1)S(1)} %convert_element_type.80), channel_id=1, replica_groups=mesh['ep_0'=16,'ep_1'=4,'ep_2'=2,'tp'=4] {'ep_1'}, dimensions={0}, use_global_device_ids=true | all-gather | bytes 20480 | tf_op jit(solution)/shard_map/all_gather | solution.py:21
  124.9 20.2 %all-gather.3 = bf16[64,4,512]{2,1,0:T(4,128)(2,1)S(1)} all-gather(bf16[4,4,512]{2,1,0:T(4,128)(2,1)S(1)} %all_gather.43), channel_id=5, replica_groups=mesh['ep_0'=16,'ep_1'=4,'ep_2'=2,'tp'=4] {'ep_0'}, dimensions={0}, use_global_device_ids=true | all-gather | bytes 278528 | tf_op jit(solution)/shard_map/all_gather | solution.py:21
  145.1 13.3 %all-gather.4 = bf16[32,4,4,512]{3,2,1,0:T(4,128)(2,1)S(1)} all-gather(bf16[16,4,4,512]{3,2,1,0:T(4,128)(2,1)S(1)} %bitcast.71), channel_id=6, replica_groups=mesh['ep_0'=16,'ep_1'=4,'ep_2'=2,'tp'=4] {'ep_2'}, dimensions={0}, use_global_device_ids=true | all-gather | bytes 786432 | tf_op jit(solution)/shard_map/all_gather | solution.py:21
  160.4 9.0 %all-to-all-start.2 = ((bf16[128,4,16]{2,1,0:T(4,128)(2,1)}), bf16[128,4,16]{2,1,0:T(4,128)(2,1)S(1)}, u32[]{:S(2)}, u32[]{:S(2)}) async-start(bf16[128,4,16]{2,1,0:T(4,128)(2,1)} %bitcast.15), calls=%async_computation.2 | async-start | bytes 262144 | tf_op jit(solution)/shard_map/all_to_all | solution.py:103
  169.5 17.1 %all-to-all-done.2 = bf16[128,4,16]{2,1,0:T(4,128)(2,1)S(1)} async-done(((bf16[128,4,16]{2,1,0:T(4,128)(2,1)}), bf16[128,4,16]{2,1,0:T(4,128)(2,1)S(1)}, u32[]{:S(2)}, u32[]{:S(2)}) %all-to-all-start.2) | async-done | bytes 16416 | tf_op jit(solution)/shard_map/all_to_all | solution.py:103
  187.3 3.2 all-to-all-start.3
  190.7 4.0 %all-to-all-done.3 = bf16[4,4,512]{2,1,0:T(4,128)(2,1)S(1)} async-done(((bf16[4,4,512]{2,1,0:T(4,128)(2,1)}), bf16[4,4,512]{2,1,0:T(4,128)(2,1)S(1)}, u32[]{:S(2)}, u32[]{:S(2)}) %all-to-all-start.3) | async-done | bytes 16416 | tf_op jit(solution)/shard_map/all_to_all | solution.py:45
  194.9 6.9 %psum.15 = f32[4]{0:T(128)S(1)} all-reduce(f32[4]{0:T(128)S(1)} %fusion.26), channel_id=1, replica_groups=mesh['ep_0'=16,'ep_1'=4,'ep_2'=2,'tp'=4] {'tp'}, use_global_device_ids=true, to_apply=%region_9.10 | all-reduce | flops 4 | bytes 32 | tf_op jit(solution)/shard_map/psum | solution.py:121
  202.4 31.9 %all_to_all.54 = bf16[128,2,512]{2,1,0:T(2,128)(2,1)} all-to-all(bf16[128,2,512]{2,1,0:T(2,128)(2,1)S(1)} %copy.132), channel_id=1, replica_groups=mesh['ep_0'=16,'ep_1'=4,'ep_2'=2,'tp'=4] {'ep_0','ep_1','ep_2'}, dimensions={0} | all-to-all | bytes 524288 | tf_op jit(solution)/shard_map/all_to_all | solution.py:128
  234.4 20.6 %all-gather.8.cloned.1.call-done = bf16[128,2,2048]{2,1,0:T(2,128)(2,1)} async-done(((bf16[128,2,512]{2,1,0:T(2,128)(2,1)}), bf16[128,2,2048]{2,1,0:T(2,128)(2,1)}) %all-gather.8.cloned.1.call-update) | async-done | bytes 1048592 | tf_op jit(solution)/shard_map/all_gather | solution.py:129
  255.0 1.5 reshape.121
  257.5 1.4 convolution_convert_fusion
  259.0 16.2 %all_to_all.55 = bf16[4,256,512]{2,1,0:T(8,128)(2,1)S(1)} all-to-all(bf16[4,256,512]{2,1,0:T(8,128)(2,1)S(1)} %bitcast.67), channel_id=1, replica_groups=mesh['ep_0'=16,'ep_1'=4,'ep_2'=2,'tp'=4] {'tp'}, dimensions={0} | all-to-all | bytes 2097152 | tf_op jit(solution)/shard_map/all_to_all | solution.py:45
  275.5 41.7 %all_to_all.56 = bf16[128,2,512]{2,1,0:T(2,128)(2,1)S(1)} all-to-all(bf16[128,2,512]{2,1,0:T(2,128)(2,1)S(1)} %convert_element_type.93), channel_id=1, replica_groups=mesh['ep_0'=16,'ep_1'=4,'ep_2'=2,'tp'=4] {'ep_0','ep_1','ep_2'}, dimensions={0} | all-to-all | bytes 524288 | tf_op jit(solution)/shard_map/all_to_all | solution.py:136
  (90 shorter events, 15.4 us)
Async XLA Ops:
  7.2 249.8 %copy-start = (bf16[1,112,2048]{2,1,0:T(8,128)(2,1)S(1)}, bf16[1,112,2048]{2,1,0:T(8,128)(2,1)}, u32[]{:S(2)}) copy-start(bf16[1,112,2048]{2,1,0:T(8,128)(2,1)} %param.29) | copy-start | bytes 1376260
  70.0 0.8 copy-start.7
  70.0 0.8 copy-start.8
  70.0 0.8 copy-start.9
  70.8 13.4 %copy-start.10 = (s32[4,2]{0,1:T(2,128)S(1)}, s32[4,2]{0,1:T(2,128)}, u32[]{:S(2)}) copy-start(s32[4,2]{0,1:T(2,128)} %param.25) | copy-start | bytes 100
  70.8 13.5 %copy-start.14 = (bf16[128]{0:T(256)(128)(2,1)S(1)}, bf16[128]{0:T(256)(128)(2,1)}, u32[]{:S(2)}) copy-start(bf16[128]{0:T(256)(128)(2,1)} %param.21) | copy-start | bytes 772
  70.9 13.5 %copy-start.11 = (f32[512]{0:T(512)S(1)}, f32[512]{0:T(512)}, u32[]{:S(2)}) copy-start(f32[512]{0:T(512)} %param.20) | copy-start | bytes 6148
  72.2 29.1 %all-to-all-start = ((f32[128,1,192]{2,1,0:T(1,128)}), f32[128,1,192]{2,1,0:T(1,128)S(1)}, u32[]{:S(2)}, u32[]{:S(2)}) async-start(f32[128,1,192]{2,1,0:T(1,128)} %reshape.148), calls=%async_computation | async-start | bytes 262144 | tf_op jit(solution)/shard_map/all_to_all | solution.py:81
  103.0 10.0 %copy-start.2 = (f32[4,4,128,128]{3,2,1,0:T(8,128)S(1)}, f32[4,4,128,128]{3,2,1,0:T(8,128)}, u32[]{:S(2)}) copy-start(f32[4,4,128,128]{3,2,1,0:T(8,128)} %param.23) | copy-start | bytes 3145732
  103.9 7.9 %all-to-all-start.1 = ((f32[4,4,1536]{2,1,0:T(4,128)}), f32[4,4,1536]{2,1,0:T(4,128)S(1)}, u32[]{:S(2)}, u32[]{:S(2)}) async-start(f32[4,4,1536]{2,1,0:T(4,128)} %copy.124), calls=%async_computation.1 | async-start | bytes 196608 | tf_op jit(solution)/shard_map/all_to_all | solution.py:39
  113.6 1.0 copy-start.1
  158.7 0.7 copy-start.6
  159.1 31.5 %copy-start.12 = (f32[4,2]{0,1:T(2,128)S(1)}, f32[4,2]{0,1:T(2,128)}, u32[]{:S(2)}) copy-start(f32[4,2]{0,1:T(2,128)} %param.26) | copy-start | bytes 100
  159.1 35.6 %copy-start.5 = (bf16[4,512]{1,0:T(4,128)(2,1)S(1)}, bf16[4,512]{1,0:T(4,128)(2,1)}, u32[]{:S(2)}) copy-start(bf16[4,512]{1,0:T(4,128)(2,1)} %param.15) | copy-start | bytes 12292
  159.2 35.8 %copy-start.13 = (bf16[512]{0:T(512)(128)(2,1)S(1)}, bf16[512]{0:T(512)(128)(2,1)}, u32[]{:S(2)}) copy-start(bf16[512]{0:T(512)(128)(2,1)} %param.24) | copy-start | bytes 3076
  160.4 26.1 %all-to-all-start.2 = ((bf16[128,4,16]{2,1,0:T(4,128)(2,1)}), bf16[128,4,16]{2,1,0:T(4,128)(2,1)S(1)}, u32[]{:S(2)}, u32[]{:S(2)}) async-start(bf16[128,4,16]{2,1,0:T(4,128)(2,1)} %bitcast.15), calls=%async_computation.2 | async-start | bytes 262144 | tf_op jit(solution)/shard_map/all_to_all | solution.py:103
  187.3 7.4 %all-to-all-start.3 = ((bf16[4,4,512]{2,1,0:T(4,128)(2,1)}), bf16[4,4,512]{2,1,0:T(4,128)(2,1)S(1)}, u32[]{:S(2)}, u32[]{:S(2)}) async-start(bf16[4,4,512]{2,1,0:T(4,128)(2,1)} %copy.131), calls=%async_computation.3 | async-start | bytes 32768 | tf_op jit(solution)/shard_map/all_to_all | solution.py:45
  190.6 64.4 %all-gather.8.cloned.1.call-start = ((), (), s32[]{:S(2)}) async-start(), calls=%async_computation.7 | async-start | bytes 1310720 | tf_op jit(solution)/shard_map/all_gather | solution.py:129
  234.4 22.1 %copy-start.4 = (bf16[1,2048,112]{1,2,0:T(8,128)(2,1)S(1)}, bf16[1,2048,112]{1,2,0:T(8,128)(2,1)}, u32[]{:S(2)}) copy-start(bf16[1,2048,112]{1,2,0:T(8,128)(2,1)} %param.27) | copy-start | bytes 1376260
  256.4 1.0 copy-start.3
Sparse Core Ops, SparseCore 0:
  234.5 20.4 all-gather.7
where the time goes:
time: 326 us; the launch traced here: 325 us
  blocking collectives  200 us (61%)
  waiting for transfers between devices  63.1 us (19%)
  starting transfers between devices  27.6 us (8%)
  between operations  14.5 us (4%)
  local copies, waits for them, and re-layouts  10.8 us (3%)
  other arithmetic  4.91 us (2%)
  matrix products  4.43 us (1%)
    all_gather x6, blocking collectives, all_blocks(): blocks = lax.all_gather(blocks, axes[k])  94.2 us
    all_to_all x1, blocking collectives, shards(): lax.all_to_all(piece_total.reshape(ep_count, capacity, -1).astype(jnp.bfl...  41.7 us
    all_to_all x1, blocking collectives, shards(): lax.all_to_all(outgoing, EP, split_axis=0, concat_axis=0, tiled=True)  31.9 us
    all_gather x1, waiting for transfers between devices, shards(): arrived = lax.all_gather(arrived_part, 'tp', axis=2, tiled=True)  20.6 us
    all_to_all x1, waiting for transfers between devices, shards(): lax.all_to_all(part_out.astype(jnp.bfloat16), EP, split_axis=0, concat_ax...  17.1 us
    all_to_all x1, waiting for transfers between devices, shards(): lax.all_to_all(partial_value, EP, split_axis=0, concat_axis=1, tiled=True)  17 us
    all_to_all x1, blocking collectives, summed_on_arrival(): lax.all_to_all(blocks, axis, split_axis=0, concat_axis=0, tiled=True)  16.2 us
    all_to_all x1, starting transfers between devices, shards(): lax.all_to_all(partial_value, EP, split_axis=0, concat_axis=1, tiled=True)  12 us
  transfers between devices with their start and end apart: 5, of which 5 were waited for; matrix products, arithmetic and copies ran while one was open for 0% of the time, Pallas kernels for 0%

commit v1 on v0

--- a/solution.py
+++ b/solution.py
@@ -126,7 +126,31 @@
         jnp.bfloat16
     )
     arrived_part = lax.all_to_all(outgoing, EP, split_axis=0, concat_axis=0, tiled=True)
-    arrived = lax.all_gather(arrived_part, "tp", axis=2, tiled=True)
+    small = lax.axis_size("tp")
+    r2 = lax.axis_index("tp")
+    k_now, item_now, arr_out = (small, r2, arrived_part.shape[2])
+    rows = []
+    for w in range(k_now):
+        rows.append((w, (w + 1) % k_now))
+    column = []
+    for w in range(k_now):
+        column.append((w, (w - 1) % k_now))
+    arrived = jnp.zeros(
+        (*arrived_part.shape[:2], k_now * arr_out, *arrived_part.shape[2 + 1 :]), arrived_part.dtype
+    )
+    arrived = lax.dynamic_update_slice_in_dim(arrived, arrived_part, item_now * arr_out, axis=2)
+    mid_arr = t1 = arrived_part
+    main = k_now // 2
+    for s in range(1, main + 1):
+        mid_arr = lax.ppermute(mid_arr, "tp", rows)
+        arrived = lax.dynamic_update_slice_in_dim(
+            arrived, mid_arr, (item_now - s) % k_now * arr_out, axis=2
+        )
+        if s < k_now - main:
+            t1 = lax.ppermute(t1, "tp", column)
+            arrived = lax.dynamic_update_slice_in_dim(
+                arrived, t1, (item_now + s) % k_now * arr_out, axis=2
+            )
     expert_rows = arrived.reshape(ep_count * capacity, model_width)
     gate_act = jnp.dot(expert_rows, w_gate[0], preferred_element_type=jnp.float32)
     up_act = jnp.dot(expert_rows, w_up[0], preferred_element_type=jnp.float32)

time: 326 us -> 301 us (0.923)
  between operations: 14.5 us -> 1.22 us
  blocking collectives: 200 us -> 188 us
  waiting for transfers between devices: 63.1 us -> 53.2 us
  starting transfers between devices: 27.6 us -> 36 us
    all_gather x1 -> x0, waiting for transfers between devices: 20.6 us -> none  [shards(): arrived = lax.all_gather(arrived_part, 'tp', axis=2, tiled=True)]
    ppermute x0 -> x3, waiting for transfers between devices: none -> 10.7 us  [the longest x2 10.7 us: shards(): mid_arr = lax.ppermute(mid_arr, 'tp', rows)]
    all_to_all x1, blocking collectives: 41.7 us -> 31.6 us  [shards(): lax.all_to_all(piece_total.reshape(ep_count, capacity, -1).astype(jnp.bfl...]
    ppermute x0 -> x3, starting transfers between devices: none -> 8.39 us  [the longest x2 4.38 us: shards(): mid_arr = lax.ppermute(mid_arr, 'tp', rows)]
  transfers between devices with their start and end apart: 5 -> 7, of which waited for: 5 -> 6; matrix products, arithmetic and copies ran while one was open for 0% -> 1% of each run, Pallas kernels for 0% -> 0%
where the time goes in v1:
time: 301 us; the launch traced here: 300 us
  blocking collectives  188 us (62%)
  waiting for transfers between devices  53.2 us (18%)
  starting transfers between devices  36 us (12%)
  local copies, waits for them, and re-layouts  10.7 us (4%)
  matrix products  5.52 us (2%)
  other arithmetic  4.91 us (2%)
    all_gather x6, blocking collectives, all_blocks(): blocks = lax.all_gather(blocks, axes[k])  94.2 us
    all_to_all x1, blocking collectives, shards(): lax.all_to_all(outgoing, EP, split_axis=0, concat_axis=0, tiled=True)  31.8 us
    all_to_all x1, blocking collectives, shards(): lax.all_to_all(piece_total.reshape(ep_count, capacity, -1).astype(jnp.bfl...  31.6 us
    all_to_all x1, waiting for transfers between devices, shards(): lax.all_to_all(part_out.astype(jnp.bfloat16), EP, split_axis=0, concat_ax...  17.1 us
    all_to_all x1, waiting for transfers between devices, shards(): lax.all_to_all(partial_value, EP, split_axis=0, concat_axis=1, tiled=True)  17 us
    all_to_all x1, blocking collectives, summed_on_arrival(): lax.all_to_all(blocks, axis, split_axis=0, concat_axis=0, tiled=True)  15.3 us
    all_to_all x1, starting transfers between devices, shards(): lax.all_to_all(partial_value, EP, split_axis=0, concat_axis=1, tiled=True)  12 us
    ppermute x2, waiting for transfers between devices, shards(): mid_arr = lax.ppermute(mid_arr, 'tp', rows)  10.7 us
  transfers between devices with their start and end apart: 7, of which 6 were waited for; matrix products, arithmetic and copies ran while one was open for 1% of the time, Pallas kernels for 0%

profile of v1, /device:TPU:33, one launch (start us, length us, event | category | flops | bytes accessed | tf_op | source)
XLA Modules:
  0.0 299.9 jit_solution(1138553459085530289)
XLA Ops:
  2.2 8.7 %psum.14 = f32[4]{0:T(128)S(1)} all-reduce(f32[4]{0:T(128)S(1)} %fusion.20), channel_id=1, replica_groups=mesh['ep_0'=16,'ep_1'=4,'ep_2'=2,'tp'=4] {'tp'}, use_global_device_ids=true, to_apply=%region_1.0 | all-reduce | flops 4 | bytes 32 | tf_op jit(solution)/shard_map/psum | solution.py:73
  11.7 9.5 %all-gather.5 = bf16[4,4,512]{2,1,0:T(4,128)(2,1)S(1)} all-gather(bf16[1,4,512]{2,1,0:T(4,128)(2,1)S(1)} %fusion.29), channel_id=2, replica_groups=mesh['ep_0'=16,'ep_1'=4,'ep_2'=2,'tp'=4] {'ep_1'}, dimensions={0}, use_global_device_ids=true | all-gather | bytes 20480 | tf_op jit(solution)/shard_map/all_gather | solution.py:21
  21.1 27.8 %all-gather.1 = bf16[64,4,512]{2,1,0:T(4,128)(2,1)S(1)} all-gather(bf16[4,4,512]{2,1,0:T(4,128)(2,1)S(1)} %all-gather.5), channel_id=3, replica_groups=mesh['ep_0'=16,'ep_1'=4,'ep_2'=2,'tp'=4] {'ep_0'}, dimensions={0}, use_global_device_ids=true | all-gather | bytes 278528 | tf_op jit(solution)/shard_map/all_gather | solution.py:21
  48.9 14.3 %all-gather.2 = bf16[32,4,4,512]{3,2,1,0:T(4,128)(2,1)S(1)} all-gather(bf16[16,4,4,512]{3,2,1,0:T(4,128)(2,1)S(1)} %bitcast.73), channel_id=4, replica_groups=mesh['ep_0'=16,'ep_1'=4,'ep_2'=2,'tp'=4] {'ep_2'}, dimensions={0}, use_global_device_ids=true | all-gather | bytes 786432 | tf_op jit(solution)/shard_map/all_gather | solution.py:21
  65.7 12.0 %all-to-all-start = ((f32[128,1,192]{2,1,0:T(1,128)}), f32[128,1,192]{2,1,0:T(1,128)S(1)}, u32[]{:S(2)}, u32[]{:S(2)}) async-start(f32[128,1,192]{2,1,0:T(1,128)} %reshape.148), calls=%async_computation | async-start | bytes 262144 | tf_op jit(solution)/shard_map/all_to_all | solution.py:81
  77.8 17.0 %all-to-all-done = f32[128,1,192]{2,1,0:T(1,128)S(1)} async-done(((f32[128,1,192]{2,1,0:T(1,128)}), f32[128,1,192]{2,1,0:T(1,128)S(1)}, u32[]{:S(2)}, u32[]{:S(2)}) %all-to-all-start) | async-done | bytes 98336 | tf_op jit(solution)/shard_map/all_to_all | solution.py:81
  97.4 3.3 %all-to-all-start.1 = ((f32[4,4,1536]{2,1,0:T(4,128)}), f32[4,4,1536]{2,1,0:T(4,128)S(1)}, u32[]{:S(2)}, u32[]{:S(2)}) async-start(f32[4,4,1536]{2,1,0:T(4,128)} %copy.133), calls=%async_computation.1 | async-start | bytes 196608 | tf_op jit(solution)/shard_map/all_to_all | solution.py:39
  100.9 4.4 %all-to-all-done.1 = f32[4,4,1536]{2,1,0:T(4,128)S(1)} async-done(((f32[4,4,1536]{2,1,0:T(4,128)}), f32[4,4,1536]{2,1,0:T(4,128)S(1)}, u32[]{:S(2)}, u32[]{:S(2)}) %all-to-all-start.1) | async-done | bytes 98336 | tf_op jit(solution)/shard_map/all_to_all | solution.py:39
  109.2 9.1 %all_gather.40 = bf16[4,4,512]{2,1,0:T(4,128)(2,1)S(1)} all-gather(bf16[1,4,512]{2,1,0:T(4,128)(2,1)S(1)} %convert_element_type.80), channel_id=1, replica_groups=mesh['ep_0'=16,'ep_1'=4,'ep_2'=2,'tp'=4] {'ep_1'}, dimensions={0}, use_global_device_ids=true | all-gather | bytes 20480 | tf_op jit(solution)/shard_map/all_gather | solution.py:21
  118.3 20.2 %all-gather.3 = bf16[64,4,512]{2,1,0:T(4,128)(2,1)S(1)} all-gather(bf16[4,4,512]{2,1,0:T(4,128)(2,1)S(1)} %all_gather.40), channel_id=5, replica_groups=mesh['ep_0'=16,'ep_1'=4,'ep_2'=2,'tp'=4] {'ep_0'}, dimensions={0}, use_global_device_ids=true | all-gather | bytes 278528 | tf_op jit(solution)/shard_map/all_gather | solution.py:21
  138.5 13.3 %all-gather.4 = bf16[32,4,4,512]{3,2,1,0:T(4,128)(2,1)S(1)} all-gather(bf16[16,4,4,512]{3,2,1,0:T(4,128)(2,1)S(1)} %bitcast.74), channel_id=6, replica_groups=mesh['ep_0'=16,'ep_1'=4,'ep_2'=2,'tp'=4] {'ep_2'}, dimensions={0}, use_global_device_ids=true | all-gather | bytes 786432 | tf_op jit(solution)/shard_map/all_gather | solution.py:21
  153.9 9.0 %all-to-all-start.2 = ((bf16[128,4,16]{2,1,0:T(4,128)(2,1)}), bf16[128,4,16]{2,1,0:T(4,128)(2,1)S(1)}, u32[]{:S(2)}, u32[]{:S(2)}) async-start(bf16[128,4,16]{2,1,0:T(4,128)(2,1)} %bitcast.15), calls=%async_computation.2 | async-start | bytes 262144 | tf_op jit(solution)/shard_map/all_to_all | solution.py:103
  162.9 17.1 %all-to-all-done.2 = bf16[128,4,16]{2,1,0:T(4,128)(2,1)S(1)} async-done(((bf16[128,4,16]{2,1,0:T(4,128)(2,1)}), bf16[128,4,16]{2,1,0:T(4,128)(2,1)S(1)}, u32[]{:S(2)}, u32[]{:S(2)}) %all-to-all-start.2) | async-done | bytes 16416 | tf_op jit(solution)/shard_map/all_to_all | solution.py:103
  180.8 3.2 %all-to-all-start.3 = ((bf16[4,4,512]{2,1,0:T(4,128)(2,1)}), bf16[4,4,512]{2,1,0:T(4,128)(2,1)S(1)}, u32[]{:S(2)}, u32[]{:S(2)}) async-start(bf16[4,4,512]{2,1,0:T(4,128)(2,1)} %copy.140), calls=%async_computation.3 | async-start | bytes 32768 | tf_op jit(solution)/shard_map/all_to_all | solution.py:45
  184.1 4.1 %all-to-all-done.3 = bf16[4,4,512]{2,1,0:T(4,128)(2,1)S(1)} async-done(((bf16[4,4,512]{2,1,0:T(4,128)(2,1)}), bf16[4,4,512]{2,1,0:T(4,128)(2,1)S(1)}, u32[]{:S(2)}, u32[]{:S(2)}) %all-to-all-start.3) | async-done | bytes 16416 | tf_op jit(solution)/shard_map/all_to_all | solution.py:45
  188.4 6.9 %psum.15 = f32[4]{0:T(128)S(1)} all-reduce(f32[4]{0:T(128)S(1)} %fusion.24), channel_id=1, replica_groups=mesh['ep_0'=16,'ep_1'=4,'ep_2'=2,'tp'=4] {'tp'}, use_global_device_ids=true, to_apply=%region_9.10 | all-reduce | flops 4 | bytes 32 | tf_op jit(solution)/shard_map/psum | solution.py:121
  195.8 31.8 %all_to_all.54 = bf16[128,2,512]{2,1,0:T(2,128)(2,1)S(1)} all-to-all(bf16[128,2,512]{2,1,0:T(2,128)(2,1)S(1)} %copy.141), channel_id=1, replica_groups=mesh['ep_0'=16,'ep_1'=4,'ep_2'=2,'tp'=4] {'ep_0','ep_1','ep_2'}, dimensions={0} | all-to-all | bytes 524288 | tf_op jit(solution)/shard_map/all_to_all | solution.py:128
  227.7 2.5 collective-permute-start
  230.1 4.0 %collective-permute-start.1 = (bf16[128,2,512]{2,1,0:T(2,128)(2,1)S(1)}, bf16[128,2,512]{2,1,0:T(2,128)(2,1)S(1)}, u32[]{:S(2)}, u32[]{:S(2)}) collective-permute-start(bf16[128,2,512]{2,1,0:T(2,128)(2,1)S(1)} %all_to_all.54), channel_id=1, source_target_pairs={{0,3},{1,0},{2,1},{3,2},{4,7},{5,4},{6,5},{7,6},{8,11},{9,8},{10,9... | collective-permute-start | bytes 786440 | tf_op jit(solution)/shard_map/ppermute | solution.py:150
  234.2 4.1 %collective-permute-done = bf16[128,2,512]{2,1,0:T(2,128)(2,1)S(1)} collective-permute-done((bf16[128,2,512]{2,1,0:T(2,128)(2,1)S(1)}, bf16[128,2,512]{2,1,0:T(2,128)(2,1)S(1)}, u32[]{:S(2)}, u32[]{:S(2)}) %collective-permute-start) | collective-permute-done | bytes 262176 | tf_op jit(solution)/shard_map/ppermute | solution.py:145
  238.3 1.9 collective-permute-start.2
  241.5 6.6 %collective-permute-done.2 = bf16[128,2,512]{2,1,0:T(2,128)(2,1)S(1)} collective-permute-done((bf16[128,2,512]{2,1,0:T(2,128)(2,1)S(1)}, bf16[128,2,512]{2,1,0:T(2,128)(2,1)S(1)}, u32[]{:S(2)}, u32[]{:S(2)}) %collective-permute-start.2) | collective-permute-done | bytes 262176 | tf_op jit(solution)/shard_map/ppermute | solution.py:145
  251.9 15.3 %all_to_all.55 = bf16[4,256,512]{2,1,0:T(8,128)(2,1)S(1)} all-to-all(bf16[4,256,512]{2,1,0:T(8,128)(2,1)S(1)} %bitcast.70), channel_id=1, replica_groups=mesh['ep_0'=16,'ep_1'=4,'ep_2'=2,'tp'=4] {'tp'}, dimensions={0} | all-to-all | bytes 2097152 | tf_op jit(solution)/shard_map/all_to_all | solution.py:45
  267.5 31.6 %all_to_all.56 = bf16[128,2,512]{2,1,0:T(2,128)(2,1)S(1)} all-to-all(bf16[128,2,512]{2,1,0:T(2,128)(2,1)S(1)} %convert_element_type.93), channel_id=1, replica_groups=mesh['ep_0'=16,'ep_1'=4,'ep_2'=2,'tp'=4] {'ep_0','ep_1','ep_2'}, dimensions={0} | all-to-all | bytes 524288 | tf_op jit(solution)/shard_map/all_to_all | solution.py:160
  (96 shorter events, 21.1 us)
Async XLA Ops:
  0.6 249.7 %copy-start = (bf16[1,112,2048]{2,1,0:T(8,128)(2,1)S(1)}, bf16[1,112,2048]{2,1,0:T(8,128)(2,1)}, u32[]{:S(2)}) copy-start(bf16[1,112,2048]{2,1,0:T(8,128)(2,1)} %param.29) | copy-start | bytes 1376260
  63.5 0.8 copy-start.6
  63.5 0.8 copy-start.7
  63.5 0.8 copy-start.8
  64.3 13.4 %copy-start.9 = (s32[4,2]{0,1:T(2,128)S(1)}, s32[4,2]{0,1:T(2,128)}, u32[]{:S(2)}) copy-start(s32[4,2]{0,1:T(2,128)} %param.25) | copy-start | bytes 100
  64.3 13.5 %copy-start.13 = (bf16[128]{0:T(256)(128)(2,1)S(1)}, bf16[128]{0:T(256)(128)(2,1)}, u32[]{:S(2)}) copy-start(bf16[128]{0:T(256)(128)(2,1)} %param.21) | copy-start | bytes 772
  64.3 13.5 %copy-start.10 = (f32[512]{0:T(512)S(1)}, f32[512]{0:T(512)}, u32[]{:S(2)}) copy-start(f32[512]{0:T(512)} %param.20) | copy-start | bytes 6148
  65.7 29.1 %all-to-all-start = ((f32[128,1,192]{2,1,0:T(1,128)}), f32[128,1,192]{2,1,0:T(1,128)S(1)}, u32[]{:S(2)}, u32[]{:S(2)}) async-start(f32[128,1,192]{2,1,0:T(1,128)} %reshape.148), calls=%async_computation | async-start | bytes 262144 | tf_op jit(solution)/shard_map/all_to_all | solution.py:81
  96.5 10.0 %copy-start.2 = (f32[4,4,128,128]{3,2,1,0:T(8,128)S(1)}, f32[4,4,128,128]{3,2,1,0:T(8,128)}, u32[]{:S(2)}) copy-start(f32[4,4,128,128]{3,2,1,0:T(8,128)} %param.23) | copy-start | bytes 3145732
  97.4 7.9 %all-to-all-start.1 = ((f32[4,4,1536]{2,1,0:T(4,128)}), f32[4,4,1536]{2,1,0:T(4,128)S(1)}, u32[]{:S(2)}, u32[]{:S(2)}) async-start(f32[4,4,1536]{2,1,0:T(4,128)} %copy.133), calls=%async_computation.1 | async-start | bytes 196608 | tf_op jit(solution)/shard_map/all_to_all | solution.py:39
  107.1 1.0 copy-start.1
  152.1 0.7 copy-start.5
  152.6 31.5 %copy-start.11 = (f32[4,2]{0,1:T(2,128)S(1)}, f32[4,2]{0,1:T(2,128)}, u32[]{:S(2)}) copy-start(f32[4,2]{0,1:T(2,128)} %param.26) | copy-start | bytes 100
  152.6 35.6 %copy-start.4 = (bf16[4,512]{1,0:T(4,128)(2,1)S(1)}, bf16[4,512]{1,0:T(4,128)(2,1)}, u32[]{:S(2)}) copy-start(bf16[4,512]{1,0:T(4,128)(2,1)} %param.15) | copy-start | bytes 12292
  152.6 35.8 %copy-start.12 = (bf16[512]{0:T(512)(128)(2,1)S(1)}, bf16[512]{0:T(512)(128)(2,1)}, u32[]{:S(2)}) copy-start(bf16[512]{0:T(512)(128)(2,1)} %param.24) | copy-start | bytes 3076
  153.9 26.1 %all-to-all-start.2 = ((bf16[128,4,16]{2,1,0:T(4,128)(2,1)}), bf16[128,4,16]{2,1,0:T(4,128)(2,1)S(1)}, u32[]{:S(2)}, u32[]{:S(2)}) async-start(bf16[128,4,16]{2,1,0:T(4,128)(2,1)} %bitcast.15), calls=%async_computation.2 | async-start | bytes 262144 | tf_op jit(solution)/shard_map/all_to_all | solution.py:103
  180.8 7.4 %all-to-all-start.3 = ((bf16[4,4,512]{2,1,0:T(4,128)(2,1)}), bf16[4,4,512]{2,1,0:T(4,128)(2,1)S(1)}, u32[]{:S(2)}, u32[]{:S(2)}) async-start(bf16[4,4,512]{2,1,0:T(4,128)(2,1)} %copy.140), calls=%async_computation.3 | async-start | bytes 32768 | tf_op jit(solution)/shard_map/all_to_all | solution.py:45
  227.7 10.6 %collective-permute-start = (bf16[128,2,512]{2,1,0:T(2,128)(2,1)S(1)}, bf16[128,2,512]{2,1,0:T(2,128)(2,1)S(1)}, u32[]{:S(2)}, u32[]{:S(2)}) collective-permute-start(bf16[128,2,512]{2,1,0:T(2,128)(2,1)S(1)} %all_to_all.54), channel_id=1, source_target_pairs={{0,1},{1,2},{2,3},{3,0},{4,5},{5,6},{6,7},{7,4},{8,9},{9,10},{10,1... | collective-permute-start | bytes 786440 | tf_op jit(solution)/shard_map/ppermute | solution.py:145
  230.1 11.1 %collective-permute-start.1 = (bf16[128,2,512]{2,1,0:T(2,128)(2,1)S(1)}, bf16[128,2,512]{2,1,0:T(2,128)(2,1)S(1)}, u32[]{:S(2)}, u32[]{:S(2)}) collective-permute-start(bf16[128,2,512]{2,1,0:T(2,128)(2,1)S(1)} %all_to_all.54), channel_id=1, source_target_pairs={{0,3},{1,0},{2,1},{3,2},{4,7},{5,4},{6,5},{7,6},{8,11},{9,8},{10,9... | collective-permute-start | bytes 786440 | tf_op jit(solution)/shard_map/ppermute | solution.py:150
  238.3 9.8 %collective-permute-start.2 = (bf16[128,2,512]{2,1,0:T(2,128)(2,1)S(1)}, bf16[128,2,512]{2,1,0:T(2,128)(2,1)S(1)}, u32[]{:S(2)}, u32[]{:S(2)}) collective-permute-start(bf16[128,2,512]{2,1,0:T(2,128)(2,1)S(1)} %collective-permute-done), channel_id=1, source_target_pairs={{0,1},{1,2},{2,3},{3,0},{4,5},{5,6},{6,7},{7,4},{8,9},{9,10},{10,1... | collective-permute-start | bytes 786440 | tf_op jit(solution)/shard_map/ppermute | solution.py:145
  248.8 1.6 copy-start.3
